TPU v7x, 32 devices: a whole 2x2x4 slice. The times are simulated.
32 devices in a mesh: sp: 4 (over z), tp: 2 (over y), dp: 4 (over x, core).
Axes of the slice: x: 2, y: 2, z: 4, core: 2. Of those that a mesh axis runs over, the one named last changes fastest.
Arguments:
- latents: bfloat16 [4, 2048, 3072], P('dp', ('sp', 'tp')), may hold values from -5 to 5
- condition: bfloat16 [4, 3072], P('dp', ('sp', 'tp')), may hold values from -6 to 6
- context: bfloat16 [4, 384, 3072], P('dp', ('sp', 'tp')), may hold values from -6 to 6
- context_cond: bfloat16 [3072], P(('sp', 'tp')), may hold values from -6 to 6
- shift_weight: bfloat16 [3072, 3072], P(('sp', 'tp')), may hold values from -0.109375 to 0.109375
- scale_weight: bfloat16 [3072, 3072], P(('sp', 'tp')), may hold values from -0.109375 to 0.109375
- out_gate_weight: bfloat16 [3072, 3072], P(('sp', 'tp')), may hold values from -0.109375 to 0.109375
- pre_gain: float32 [3072], replicated, may hold values from 0.1 to 1.9
- post_gain: float32 [3072], replicated, may hold values from 0.1 to 1.9
- query_weight: bfloat16 [3072, 1024], P(None, 'tp'), may hold values from -0.108253175 to 0.108253175
- key_weight: bfloat16 [3072, 256], replicated, may hold values from -0.108253175 to 0.108253175
- value_weight: bfloat16 [3072, 256], replicated, may hold values from -0.109375 to 0.109375
- head_gate_weight: bfloat16 [3072, 1024], P(None, 'tp'), may hold values from -0.109375 to 0.109375
- lambdas: float32 [8], P('tp'), may hold values from 0.3 to 0.8
- head_gain: float32 [128], replicated, may hold values from 0.1 to 1.9
- out_weight: bfloat16 [1024, 3072], P(None, 'tp'), may hold values from -0.1875 to 0.1875
Outputs:
- mixed_out: bfloat16 [4, 2048, 3072], P('dp', ('sp', 'tp'))
All inputs are finite; a program needn't handle non-finite values.
Results may differ from a plain program's by a relative error of at most 0.0128.
The roundings to bfloat16 on the way count: a program that leaves them out, or rounds other values in their place, can miss the bound.
Values may be sent and summed in bfloat16 or wider, within the bound.
A program may use at most 64 MiB of HBM per device.

v0:
```python
import functools
import math

import jax
import jax.numpy as jnp
from jax import lax
from jax.experimental import pallas as pl
from jax.experimental.pallas import tpu as pltpu
from jax.sharding import PartitionSpec as P


HEADS = 8
KVH = 2
HQK = 64
HV = 128
NORM_EPSILON = 1e-06
MESH = pl.DeviceIdType.MESH


def norm_rows(values, norm_gain):
    return (
        values
        * lax.rsqrt(jnp.mean(values * values, axis=-1, keepdims=True) + NORM_EPSILON)
        * norm_gain
    )


def modulate(tokens, norm_gain, shift, scale):
    values = norm_rows(tokens.astype(jnp.float32), norm_gain)
    return (values * (1.0 + scale) + shift).astype(jnp.bfloat16)


def project(tokens, weight):
    return jnp.dot(tokens, weight, preferred_element_type=jnp.float32).astype(jnp.bfloat16)


def shifted(values, axis, size, step):
    return lax.ppermute(values, axis, [(i, (i + step) % size) for i in range(size)])


def peer(offset, sp, tp):
    me = lax.axis_index("sp") * tp + lax.axis_index("tp")
    other = lax.rem(me + offset, sp * tp)
    return other // tp, lax.rem(other, tp)


def enter(sp, tp):
    barrier = pltpu.get_barrier_semaphore()
    for offset in range(1, sp * tp):
        row, column = peer(offset, sp, tp)
        pl.semaphore_signal(
            barrier, inc=1, device_id={"sp": row, "tp": column}, device_id_type=MESH
        )
    pl.semaphore_wait(barrier, sp * tp - 1)


def sum_kernel(sp, tp, part_ref, total_ref, held, send_sem, recv_sem):
    enter(sp, tp)
    copies = []
    for offset in range(1, sp * tp):
        row, column = peer(offset, sp, tp)
        copy = pltpu.make_async_remote_copy(
            src_ref=part_ref,
            dst_ref=held.at[offset - 1],
            send_sem=send_sem.at[offset - 1],
            recv_sem=recv_sem.at[offset - 1],
            device_id={"sp": row, "tp": column},
            device_id_type=MESH,
        )
        copy.start()
        copies.append(copy)
    total = part_ref[...]
    for offset, copy in enumerate(copies):
        copy.wait_recv()
        total = total + held[offset]
    total_ref[...] = total
    for copy in copies:
        copy.wait_send()


def sum_over_group(parts, sp, tp):
    others = sp * tp - 1
    return pl.pallas_call(
        functools.partial(sum_kernel, sp, tp),
        out_shape=jax.ShapeDtypeStruct(parts.shape, parts.dtype),
        in_specs=[pl.BlockSpec(memory_space=pltpu.VMEM)],
        out_specs=pl.BlockSpec(memory_space=pltpu.VMEM),
        scratch_shapes=[
            pltpu.VMEM((others,) + parts.shape, parts.dtype),
            pltpu.SemaphoreType.DMA((others,)),
            pltpu.SemaphoreType.DMA((others,)),
        ],
        compiler_params=pltpu.CompilerParams(collective_id=0, has_side_effects=True),
        cost_estimate=pl.CostEstimate(flops=10**6, bytes_accessed=20 * 10**6, transcendentals=0),
    )(parts)


def attend_kernel(count, lambda_ref, q_ref, gate_ref, gain_ref, *refs):
    key_refs, value_refs, out_ref = refs[:count], refs[count : 2 * count], refs[2 * count]
    queries = q_ref[...]
    rows = queries.shape[0]
    lane = lax.broadcasted_iota(jnp.int32, queries.shape, 1)
    queries = (queries.astype(jnp.float32) * HQK ** (-0.5))
    both = jnp.concatenate(
        [jnp.where(lane < HQK, queries, 0.0), jnp.where(lane < HQK, 0.0, queries)], axis=0
    ).astype(jnp.bfloat16)
    contract = (((1,), (1,)), ((), ()))
    keys = jnp.concatenate([ref[...] for ref in key_refs], axis=0)
    values = jnp.concatenate([ref[...] for ref in value_refs], axis=0)
    scores = lax.dot_general(both, keys, contract, preferred_element_type=jnp.float32)
    largest = jnp.max(scores, axis=-1, keepdims=True)
    exponent = jnp.exp(scores - largest)
    normalizer = jnp.sum(exponent, axis=-1, keepdims=True)
    weighted = jnp.dot(exponent.astype(jnp.bfloat16), values, preferred_element_type=jnp.float32)
    ratios = weighted / normalizer
    attended = ratios[:rows] - lambda_ref[pl.program_id(0)] * ratios[rows:]
    gate = jax.nn.silu(gate_ref[...].astype(jnp.float32))
    out_ref[...] = (norm_rows(attended, gain_ref[...]) * gate).astype(jnp.bfloat16)


def attend(lambdas, queries, gate, head_gain, parts):
    rows, width = queries.shape
    heads = width // (2 * HQK)
    block = math.gcd(rows, 128)
    keys = sum(part.shape[0] for part in parts)

    def whole(part, column):
        return pl.BlockSpec((part.shape[0], 128), lambda h, i: (0, column))

    tile = pl.BlockSpec((block, 128), lambda h, i: (i, h))
    return pl.pallas_call(
        functools.partial(attend_kernel, len(parts)),
        grid=(heads, rows // block),
        out_shape=jax.ShapeDtypeStruct((rows, heads * HV), jnp.bfloat16),
        in_specs=[
            pl.BlockSpec(memory_space=pltpu.SMEM),
            tile,
            tile,
            pl.BlockSpec((1, HV), lambda h, i: (0, 0)),
            *(whole(part, 0) for part in parts),
            *(whole(part, 1) for part in parts),
        ],
        out_specs=tile,
        compiler_params=pltpu.CompilerParams(vmem_limit_bytes=48 * 2**20),
        cost_estimate=pl.CostEstimate(
            flops=16 * heads * rows * keys * HV, bytes_accessed=4 * 10**6,
            transcendentals=2 * heads * rows * keys,
        ),
    )(lambdas, queries, gate, head_gain, *parts, *parts)


def tail_kernel(tp, dp, *refs):
    branches, refs = refs[:tp], refs[tp:]
    own_weight, refs = refs[0], refs[1:]
    pieces, refs = refs[: (tp - 1) * dp], refs[(tp - 1) * dp :]
    out_gate_ref, gain_ref, out_ref, branch, projected = refs
    me, mine = lax.axis_index("tp"), lax.axis_index("dp")
    width = branches[0].shape[1]
    columns = own_weight.shape[1]
    depth = own_weight.shape[0] // dp
    for step in range(tp):
        owner = lax.rem(me + step, tp)
        branch[:, pl.ds(pl.multiple_of(owner * width, width), width)] = branches[step][...]
    projected[:, pl.ds(pl.multiple_of(me * columns, columns), columns)] = jnp.dot(
        branch[...], own_weight[...], preferred_element_type=jnp.float32
    )
    for step in range(1, tp):
        owner = lax.rem(me - step + tp, tp)
        total = None
        for turn in range(dp):
            source = lax.bitwise_xor(mine, turn)
            part = jnp.dot(
                branch[:, pl.ds(pl.multiple_of(source * depth, depth), depth)],
                pieces[(step - 1) * dp + turn][...],
                preferred_element_type=jnp.float32,
            )
            total = part if total is None else total + part
        projected[:, pl.ds(pl.multiple_of(owner * columns, columns), columns)] = total
    values = projected[...].astype(jnp.bfloat16).astype(jnp.float32)
    out_ref[...] = (out_gate_ref[...] * norm_rows(values, gain_ref[...])).astype(jnp.bfloat16)


def tail(branches, own_weight, pieces, out_gate, post_gain, tp, dp):
    rows = branches[0].shape[0]
    width = post_gain.shape[1]
    operands = (*branches, own_weight, *pieces, out_gate, post_gain)
    return pl.pallas_call(
        functools.partial(tail_kernel, tp, dp),
        out_shape=jax.ShapeDtypeStruct((rows, width), jnp.bfloat16),
        in_specs=[pl.BlockSpec(memory_space=pltpu.VMEM)] * len(operands),
        out_specs=pl.BlockSpec(memory_space=pltpu.VMEM),
        scratch_shapes=[
            pltpu.VMEM((rows, own_weight.shape[0]), jnp.bfloat16),
            pltpu.VMEM((rows, width), jnp.float32),
        ],
        compiler_params=pltpu.CompilerParams(vmem_limit_bytes=48 * 2**20),
        cost_estimate=pl.CostEstimate(
            flops=2 * rows * width * own_weight.shape[0], bytes_accessed=10**7, transcendentals=0
        ),
    )(*operands)


def local(
    sp,
    tp,
    dp,
    latents,
    condition,
    context,
    context_cond,
    shift_weight,
    scale_weight,
    out_gate_weight,
    pre_gain,
    post_gain,
    query_weight,
    key_weight,
    value_weight,
    head_gate_weight,
    lambdas,
    head_gain,
    out_weight,
):
    pair_width = 2 * HQK
    local_heads = query_weight.shape[1] // pair_width
    per_group = (HEADS // KVH) // local_heads
    key_group = lax.axis_index("tp") // per_group
    own = latents[0]
    rows = own.shape[0]
    early = rows // 4
    steps = range(1, tp)
    heads_up = [shifted(own[:early], "tp", tp, step) for step in steps]

    conditions = jnp.concatenate([condition, context_cond[None, :]], axis=0).astype(jnp.float32)
    conditions = jax.nn.silu(conditions).astype(jnp.bfloat16)
    parts = jnp.concatenate(
        [
            jnp.dot(conditions, shift_weight, preferred_element_type=jnp.float32),
            jnp.dot(conditions, scale_weight, preferred_element_type=jnp.float32),
            jnp.dot(conditions[:1], out_gate_weight, preferred_element_type=jnp.float32),
        ],
        axis=0,
    )
    sums = sum_over_group(parts, sp, tp)
    late, sums = lax.optimization_barrier((own[early:], sums))
    shift, context_shift, scale, context_scale, out_gate = (
        sums[0:1], sums[1:2], sums[2:3], sums[3:4], sums[4:5]
    )
    rest = [shifted(late, "tp", tp, step) for step in steps]

    own_key_weight = lax.dynamic_slice_in_dim(key_weight, key_group * pair_width, pair_width, 1)
    own_value_weight = lax.dynamic_slice_in_dim(value_weight, key_group * HV, HV, 1)
    kv_weight = jnp.concatenate([own_key_weight, own_value_weight], axis=1)

    def spread(values):
        return [values] + [shifted(values, "sp", sp, step) for step in range(1, sp)]

    own_in = modulate(own, pre_gain, shift, scale)
    own_kv = project(own_in, kv_weight)
    own_kv = spread(own_kv)
    own_queries = project(own_in, query_weight)
    own_gate = project(own_in, head_gate_weight)

    context_in = modulate(context[0], pre_gain, context_shift, context_scale)
    context_kv = jnp.concatenate(
        [project(context_in, key_weight), project(context_in, value_weight)], axis=1
    )
    contexts = [context_kv] + [shifted(context_kv, "tp", tp, step) for step in steps]
    contexts = [
        jnp.concatenate(
            [
                lax.dynamic_slice_in_dim(part, key_group * pair_width, pair_width, 1),
                lax.dynamic_slice_in_dim(part, KVH * pair_width + key_group * HV, HV, 1),
            ],
            axis=1,
        )
        for part in contexts
    ]

    depth = out_weight.shape[0] // dp
    share = lax.dynamic_slice_in_dim(out_weight, lax.axis_index("dp") * depth, depth, 0)
    share, *rest = lax.optimization_barrier((share, *rest))
    pieces = []
    for step in steps:
        turns = {0: shifted(share, "tp", tp, step)}
        bit = dp // 2
        while bit:
            for turn in list(turns):
                turns[turn ^ bit] = lax.ppermute(
                    turns[turn], "dp", [(i, i ^ bit) for i in range(dp)]
                )
            bit //= 2
        pieces.extend(turns[turn] for turn in range(dp))

    other_in = modulate(
        jnp.concatenate([part for pair in zip(heads_up, rest) for part in pair], axis=0),
        pre_gain, shift, scale,
    )
    other_kv = spread(jnp.concatenate([project(other_in, kv_weight), *contexts], axis=0))
    other_queries = project(other_in, query_weight)
    other_gate = project(other_in, head_gate_weight)

    keys = own_kv + other_kv
    gain = head_gain[None, :]
    other_branch = attend(lambdas, other_queries, other_gate, gain, keys)
    returned = [
        shifted(other_branch[(step - 1) * rows : step * rows], "tp", tp, tp - step)
        for step in steps
    ]
    own_branch = attend(lambdas, own_queries, own_gate, gain, keys)
    branches = [own_branch, *returned]
    result = tail(branches, out_weight, pieces, out_gate, post_gain[None, :], tp, dp)
    return result[None]


def solution(mesh):
    return jax.shard_map(
        functools.partial(local, mesh.shape["sp"], mesh.shape["tp"], mesh.shape["dp"]),
        mesh=mesh,
        in_specs=(
            P("dp", ("sp", "tp"), None),
            P("dp", ("sp", "tp")),
            P("dp", ("sp", "tp"), None),
            P(("sp", "tp")),
            P(("sp", "tp"), None),
            P(("sp", "tp"), None),
            P(("sp", "tp"), None),
            P(),
            P(),
            P(None, "tp"),
            P(),
            P(),
            P(None, "tp"),
            P("tp"),
            P(),
            P(None, "tp"),
        ),
        out_specs=P("dp", ("sp", "tp"), None),
        check_vma=False,
    )
```

profile of v0, /device:TPU:0, one launch (start us, length us, event | category | flops | bytes accessed | tf_op | source)
XLA Modules:
  0.0 138.9 jit_solution(12878110756212739601)
XLA Ops:
  0.0 2.5 %slice_bitcast_fusion = bf16[192,3072]{1,0:T(8,128)(2,1)} fusion(bf16[1,256,3072]{2,1,0:T(8,128)(2,1)} %param.16), kind=kLoop, calls=%fused_computation.20 | loop fusion | bytes 2359296 | tf_op jit(solution)/shard_map/slice | solution.py:245
  4.2 0.5 copy-done.12
  5.2 0.7 pad_maximum_fusion.4.part_ref
  5.8 20.3 %shard_map.154 = f32[5,3072]{1,0:T(8,128)} custom-call(f32[5,3072]{1,0:T(8,128)} %pad_maximum_fusion.4.part_ref), custom_call_target="tpu_custom_call" | custom-call | flops 1000000 | bytes 20000000 | tf_op jit(solution)/shard_map/pallas_call | solution.py:83
  26.2 1.9 %fusion.31 = (f32[1,3072]{1,0:T(1,128)S(1)}, f32[1,3072]{1,0:T(1,128)}, f32[1,3072]{1,0:T(1,128)}, f32[1,3072]{1,0:T(1,128)S(1)}, f32[1,3072]{1,0:T(1,128)S(1)}) fusion(f32[5,3072]{1,0:T(8,128)} %shard_map.154), kind=kLoop, calls=%fused_computation.61 | loop fusion | flops 6144 | bytes 122880 | tf_op jit(solution)/shard_map/slice | solution.py:247
  28.0 1.6 %constant_dynamic-slice_fusion.3 = (bf16[3072,128]{1,0:T(8,128)(2,1)S(1)}, bf16[3072,128]{1,0:T(8,128)(2,1)S(1)}) fusion(bf16[3072,256]{1,0:T(8,128)(2,1)} %param.27, s32[]{:T(128)S(6)} %select_n.18, bf16[3072,256]{1,0:T(8,128)(2,1)} %param.26), kind=kLoop, calls=%fused_computation.52 | loop fusion | bytes 3145732 | tf_op jit(solution)/shard_map/dynamic_slice | solution.py:252
  29.9 0.8 convolution_convert_fusion.5.refs_0_.refs_8_
  30.8 4.8 %collective-permute-start = (bf16[256,256]{1,0:T(8,128)(2,1)S(1)}, bf16[256,256]{1,0:T(8,128)(2,1)S(1)}, u32[]{:S(2)}, u32[]{:S(2)}) collective-permute-start(bf16[256,256]{1,0:T(8,128)(2,1)S(1)} %convolution_convert_fusion.5.refs_0_.refs_8_), channel_id=1, source_target_pairs={{0,8},{8,16},{16,24},{24,0},{1,9},{9,17},{17,25},{25,1},{2,10},{10... | collective-permute-start | bytes 393224 | tf_op jit(solution)/shard_map/ppermute | solution.py:38
  35.5 2.4 %collective-permute-start.1 = (bf16[256,256]{1,0:T(8,128)(2,1)S(1)}, bf16[256,256]{1,0:T(8,128)(2,1)S(1)}, u32[]{:S(2)}, u32[]{:S(2)}) collective-permute-start(bf16[256,256]{1,0:T(8,128)(2,1)S(1)} %convolution_convert_fusion.5.refs_0_.refs_8_), channel_id=1, source_target_pairs={{0,16},{8,24},{16,0},{24,8},{1,17},{9,25},{17,1},{25,9},{2,18},{10... | collective-permute-start | bytes 393224 | tf_op jit(solution)/shard_map/ppermute | solution.py:38
  38.0 2.5 %collective-permute-start.4 = (bf16[192,3072]{1,0:T(8,128)(2,1)}, bf16[192,3072]{1,0:T(8,128)(2,1)}, u32[]{:S(2)}, u32[]{:S(2)}) collective-permute-start(bf16[192,3072]{1,0:T(8,128)(2,1)} %slice_bitcast_fusion), channel_id=1, source_target_pairs={{0,4},{4,0},{1,5},{5,1},{2,6},{6,2},{3,7},{7,3},{8,12},{12,8},{9,1... | collective-permute-start | bytes 3538952 | tf_op jit(solution)/shard_map/ppermute | solution.py:38
  40.4 0.8 slice_bitcast_fusion.1
  42.5 0.6 pad_maximum_fusion.5
  43.1 2.0 %collective-permute-start.5 = (bf16[48,512]{1,0:T(8,128)(2,1)}, bf16[48,512]{1,0:T(8,128)(2,1)}, u32[]{:S(2)}, u32[]{:S(2)}) collective-permute-start(bf16[48,512]{1,0:T(8,128)(2,1)} %pad_maximum_fusion.5), channel_id=1, source_target_pairs={{0,4},{4,0},{1,5},{5,1},{2,6},{6,2},{3,7},{7,3},{8,12},{12,8},{9,1... | collective-permute-start | bytes 147464 | tf_op jit(solution)/shard_map/ppermute | solution.py:38
  45.1 2.6 %convolution_convert_fusion.2.gate_ref = bf16[256,512]{1,0:T(8,128)(2,1)S(1)} fusion(bf16[3072,512]{1,0:T(8,128)(2,1)S(1)} %copy-done, bf16[1,256,3072]{2,1,0:T(8,128)(2,1)} %param.16, f32[3072]{0:T(1024)} %bitcast.47, f32[3072]{0:T(1024)} %bitcast.53, f32[3072]{0:T(1024)} %param.23, f32[256]{0:T(256)S(1)} %add_rsqrt_fusion.1), kind=kOutput, calls=%fused_computation.18 | convolution fusion | flops 810156032 | bytes 5018624 | tf_op jit(solution)/shard_map/dot_general | solution.py:34
  48.0 1.0 convolution_convert_fusion.3.q_ref
  49.1 1.3 constant_dynamic-slice_fusion.2
  50.5 17.1 %collective-permute-done.4 = bf16[192,3072]{1,0:T(8,128)(2,1)} collective-permute-done((bf16[192,3072]{1,0:T(8,128)(2,1)}, bf16[192,3072]{1,0:T(8,128)(2,1)}, u32[]{:S(2)}, u32[]{:S(2)}) %collective-permute-start.4) | collective-permute-done | bytes 1179680 | tf_op jit(solution)/shard_map/ppermute | solution.py:38
  67.7 6.8 %collective-permute-done.5 = bf16[48,512]{1,0:T(8,128)(2,1)} collective-permute-done((bf16[48,512]{1,0:T(8,128)(2,1)}, bf16[48,512]{1,0:T(8,128)(2,1)}, u32[]{:S(2)}, u32[]{:S(2)}) %collective-permute-start.5) | collective-permute-done | bytes 49184 | tf_op jit(solution)/shard_map/ppermute | solution.py:38
  74.5 1.8 %collective-permute-start.10 = (bf16[256,1536]{1,0:T(8,128)(2,1)S(1)}, bf16[256,1536]{1,0:T(8,128)(2,1)S(1)}, u32[]{:S(2)}, u32[]{:S(2)}) collective-permute-start(bf16[256,1536]{1,0:T(8,128)(2,1)S(1)} %constant_dynamic-slice_fusion.2), channel_id=1, source_target_pairs={{0,4},{4,0},{1,5},{5,1},{2,6},{6,2},{3,7},{7,3},{8,12},{12,8},{9,1... | collective-permute-start | bytes 2359304 | tf_op jit(solution)/shard_map/ppermute | solution.py:38
  76.2 0.7 constant_dynamic-slice_fusion.1
  77.0 1.7 %fusion = f32[256]{0:T(256)S(1)} fusion(bf16[192,3072]{1,0:T(8,128)(2,1)} %collective-permute-done.4, bf16[64,3072]{1,0:T(8,128)(2,1)} %collective-permute-done.3), kind=kLoop, calls=%fused_computation.4 | loop fusion | flops 4718336 | bytes 1573888 | tf_op jit(solution)/shard_map/reduce_sum | solution.py:23
  78.7 2.1 %convolution_convert_fusion.4 = bf16[256,256]{1,0:T(8,128)(2,1)S(1)} fusion(bf16[3072,128]{1,0:T(8,128)(2,1)S(1)} %copy-done.14, bf16[3072,128]{1,0:T(8,128)(2,1)S(1)} %copy-done.16, f32[256]{0:T(256)S(1)} %add_rsqrt_fusion, f32[3072]{0:T(1024)S(1)} %bitcast.49, f32[3072]{0:T(1024)S(1)} %bitcast.55, f32[3072]{0:T(1024)S(1)} %copy-done.25, ...), kind=kOutput, calls=%fused_computation.21 | convolution fusion | flops 412942336 | bytes 3314688 | tf_op jit(solution)/shard_map/dot_general | solution.py:34
  81.3 10.2 %collective-permute-done.10.refs_3_ = bf16[256,1536]{1,0:T(8,128)(2,1)S(1)} collective-permute-done((bf16[256,1536]{1,0:T(8,128)(2,1)S(1)}, bf16[256,1536]{1,0:T(8,128)(2,1)S(1)}, u32[]{:S(2)}, u32[]{:S(2)}) %collective-permute-start.10) | collective-permute-done | bytes 786464 | tf_op jit(solution)/shard_map/ppermute | solution.py:38
  91.5 1.5 %collective-permute-start.12 = (bf16[256,1536]{1,0:T(8,128)(2,1)S(1)}, bf16[256,1536]{1,0:T(8,128)(2,1)S(1)}, u32[]{:S(2)}, u32[]{:S(2)}) collective-permute-start(bf16[256,1536]{1,0:T(8,128)(2,1)S(1)} %collective-permute-done.10.refs_3_), channel_id=1, source_target_pairs={{0,2},{1,3},{2,0},{3,1},{4,6},{5,7},{6,4},{7,5},{8,10},{9,11},{10,... | collective-permute-start | bytes 2359304 | tf_op jit(solution)/shard_map/ppermute | solution.py:289
  92.9 2.4 %convolution_convert_fusion.gate_ref = bf16[256,512]{1,0:T(8,128)(2,1)S(1)} fusion(bf16[3072,512]{1,0:T(8,128)(2,1)S(1)} %copy-done, f32[256]{0:T(256)S(1)} %add_rsqrt_fusion, f32[3072]{0:T(1024)S(1)} %bitcast.50, f32[3072]{0:T(1024)S(1)} %bitcast.56, f32[3072]{0:T(1024)S(1)} %copy-done.25, bf16[192,3072]{1,0:T(8,128)(2,1)} %collective-permute-done.4, ...), kind=kOutput, calls=%fused_computation.16 | convolution fusion | flops 812515328 | bytes 5018624 | tf_op jit(solution)/shard_map/dot_general | solution.py:34
  95.4 3.3 %collective-permute-start.7 = (bf16[352,256]{1,0:T(8,128)(2,1)S(1)}, bf16[352,256]{1,0:T(8,128)(2,1)S(1)}, u32[]{:S(2)}, u32[]{:S(2)}) collective-permute-start(bf16[352,256]{1,0:T(8,128)(2,1)S(1)} %maximum_maximum_fusion.refs_4_.refs_12_), channel_id=1, source_target_pairs={{0,16},{8,24},{16,0},{24,8},{1,17},{9,25},{17,1},{25,9},{2,18},{10... | collective-permute-start | bytes 540680 | tf_op jit(solution)/shard_map/ppermute | solution.py:38
  99.0 2.4 %convolution_convert_fusion.1.q_ref = bf16[256,512]{1,0:T(8,128)(2,1)S(1)} fusion(bf16[3072,512]{1,0:T(8,128)(2,1)S(1)} %copy-done.32, f32[256]{0:T(256)S(1)} %add_rsqrt_fusion, f32[3072]{0:T(1024)S(1)} %bitcast.51, f32[3072]{0:T(1024)S(1)} %bitcast.57, f32[3072]{0:T(1024)S(1)} %copy-done.25, bf16[192,3072]{1,0:T(8,128)(2,1)} %collective-permute-done.4, ...), kind=kOutput, calls=%fused_computation.17 | convolution fusion | flops 812515328 | bytes 5018624 | tf_op jit(solution)/shard_map/dot_general | solution.py:34
  101.5 6.1 %collective-permute-done.12.refs_5_ = bf16[256,1536]{1,0:T(8,128)(2,1)S(1)} collective-permute-done((bf16[256,1536]{1,0:T(8,128)(2,1)S(1)}, bf16[256,1536]{1,0:T(8,128)(2,1)S(1)}, u32[]{:S(2)}, u32[]{:S(2)}) %collective-permute-start.12) | collective-permute-done | bytes 786464 | tf_op jit(solution)/shard_map/ppermute | solution.py:289
  107.6 12.2 %shard_map.156 = bf16[256,512]{1,0:T(8,128)(2,1)S(1)} custom-call(f32[4]{0:T(128)S(1)} %copy-done.2, bf16[256,512]{1,0:T(8,128)(2,1)S(1)} %convolution_convert_fusion.1.q_ref, bf16[256,512]{1,0:T(8,128)(2,1)S(1)} %convolution_convert_fusion.gate_ref, f32[1,128]{1,0:T(1,128)S(1)} %bitcast.40, bf16[256,256]{1,0:T(8,128)(2,1)S(1)} %convolution_convert_fusion.5.refs_0_.refs_8_, ...), custom_call_target="tpu_custom_call" | custom-call | flops 5100273664 | bytes 4000000 | tf_op jit(solution)/shard_map/pallas_call | solution.py:131
  119.8 1.3 collective-permute-start.9
  121.1 12.1 %shard_map.155.refs_0_ = bf16[256,512]{1,0:T(8,128)(2,1)S(1)} custom-call(f32[4]{0:T(128)S(1)} %copy-done.2, bf16[256,512]{1,0:T(8,128)(2,1)S(1)} %convolution_convert_fusion.3.q_ref, bf16[256,512]{1,0:T(8,128)(2,1)S(1)} %convolution_convert_fusion.2.gate_ref, f32[1,128]{1,0:T(1,128)S(1)} %bitcast.41, ...), custom_call_target="tpu_custom_call" | custom-call | flops 5100273664 | bytes 4000000 | tf_op jit(solution)/shard_map/pallas_call | solution.py:131
  133.3 5.7 %shard_map.157 = bf16[256,3072]{1,0:T(8,128)(2,1)} custom-call(bf16[256,512]{1,0:T(8,128)(2,1)S(1)} %shard_map.155.refs_0_, bf16[256,512]{1,0:T(8,128)(2,1)S(1)} %collective-permute-done.9.refs_1_, bf16[1024,1536]{1,0:T(8,128)(2,1)} %refs_2_.1, bf16[256,1536]{1,0:T(8,128)(2,1)S(1)} %collective-permute-done.10.refs_3_, ...), custom_call_target="tpu_custom_call" | custom-call | flops 1610612736 | bytes 10000000 | tf_op jit(solution)/shard_map/pallas_call | solution.py:187
  (95 shorter events, 4.9 us)
Async XLA Ops:
  0.0 45.1 %copy-start = (bf16[3072,512]{1,0:T(8,128)(2,1)S(1)}, bf16[3072,512]{1,0:T(8,128)(2,1)}, u32[]{:S(2)}) copy-start(bf16[3072,512]{1,0:T(8,128)(2,1)} %param.28) | copy-start | bytes 9437188
  0.0 2.9 %copy-start.31 = (bf16[384]{0:T(512)(128)(2,1)S(1)}, bf16[384]{0:T(512)(128)(2,1)}, u32[]{:S(2)}) copy-start(bf16[384]{0:T(512)(128)(2,1)} %param.19) | copy-start | bytes 2308
  0.0 3.0 %copy-start.30 = (bf16[1,384]{1,0:T(2,128)(2,1)S(1)}, bf16[1,384]{1,0:T(2,128)(2,1)}, u32[]{:S(2)}) copy-start(bf16[1,384]{1,0:T(2,128)(2,1)} %param.17) | copy-start | bytes 2308
  0.0 3.1 %copy-start.10 = (bf16[384,3072]{1,0:T(8,128)(2,1)S(1)}, bf16[384,3072]{1,0:T(8,128)(2,1)}, u32[]{:S(2)}) copy-start(bf16[384,3072]{1,0:T(8,128)(2,1)} %param.20) | copy-start | bytes 7077892
  0.0 3.8 %copy-start.11 = (bf16[384,3072]{1,0:T(8,128)(2,1)S(1)}, bf16[384,3072]{1,0:T(8,128)(2,1)}, u32[]{:S(2)}) copy-start(bf16[384,3072]{1,0:T(8,128)(2,1)} %param.21) | copy-start | bytes 7077892
  4.7 24.9 %copy-start.23 = (f32[3072]{0:T(1024)S(1)}, f32[3072]{0:T(1024)}, u32[]{:S(2)}) copy-start(f32[3072]{0:T(1024)} %param.23) | copy-start | bytes 36868
  29.9 11.3 %copy-start.9 = (bf16[1,48,3072]{2,1,0:T(8,128)(2,1)S(1)}, bf16[1,48,3072]{2,1,0:T(8,128)(2,1)}, u32[]{:S(2)}) copy-start(bf16[1,48,3072]{2,1,0:T(8,128)(2,1)} %param.18) | copy-start | bytes 884740
  29.9 11.5 %copy-start.7 = (bf16[3072,256]{1,0:T(8,128)(2,1)S(1)}, bf16[3072,256]{1,0:T(8,128)(2,1)}, u32[]{:S(2)}) copy-start(bf16[3072,256]{1,0:T(8,128)(2,1)} %param.27) | copy-start | bytes 4718596
  29.9 11.5 %copy-start.21 = (f32[1,3072]{1,0:T(1,128)S(1)}, f32[1,3072]{1,0:T(1,128)}, u32[]{:S(2)}) copy-start(f32[1,3072]{1,0:T(1,128)} %get-tuple-element.14) | copy-start | bytes 36868
  29.9 11.5 %copy-start.22 = (f32[1,3072]{1,0:T(1,128)S(1)}, f32[1,3072]{1,0:T(1,128)}, u32[]{:S(2)}) copy-start(f32[1,3072]{1,0:T(1,128)} %get-tuple-element.15) | copy-start | bytes 36868
  29.9 11.5 %copy-start.24 = (f32[3072]{0:T(1024)S(1)}, f32[3072]{0:T(1024)}, u32[]{:S(2)}) copy-start(f32[3072]{0:T(1024)} %param.23) | copy-start | bytes 36868
  29.9 11.9 %copy-start.8 = (bf16[3072,256]{1,0:T(8,128)(2,1)S(1)}, bf16[3072,256]{1,0:T(8,128)(2,1)}, u32[]{:S(2)}) copy-start(bf16[3072,256]{1,0:T(8,128)(2,1)} %param.26) | copy-start | bytes 4718596
  30.8 64.6 %collective-permute-start = (bf16[256,256]{1,0:T(8,128)(2,1)S(1)}, bf16[256,256]{1,0:T(8,128)(2,1)S(1)}, u32[]{:S(2)}, u32[]{:S(2)}) collective-permute-start(bf16[256,256]{1,0:T(8,128)(2,1)S(1)} %convolution_convert_fusion.5.refs_0_.refs_8_), channel_id=1, source_target_pairs={{0,8},{8,16},{16,24},{24,0},{1,9},{9,17},{17,25},{25,1},{2,10},{10... | collective-permute-start | bytes 393224 | tf_op jit(solution)/shard_map/ppermute | solution.py:38
  35.5 63.2 %collective-permute-start.1 = (bf16[256,256]{1,0:T(8,128)(2,1)S(1)}, bf16[256,256]{1,0:T(8,128)(2,1)S(1)}, u32[]{:S(2)}, u32[]{:S(2)}) collective-permute-start(bf16[256,256]{1,0:T(8,128)(2,1)S(1)} %convolution_convert_fusion.5.refs_0_.refs_8_), channel_id=1, source_target_pairs={{0,16},{8,24},{16,0},{24,8},{1,17},{9,25},{17,1},{25,9},{2,18},{10... | collective-permute-start | bytes 393224 | tf_op jit(solution)/shard_map/ppermute | solution.py:38
  38.0 29.6 %collective-permute-start.4 = (bf16[192,3072]{1,0:T(8,128)(2,1)}, bf16[192,3072]{1,0:T(8,128)(2,1)}, u32[]{:S(2)}, u32[]{:S(2)}) collective-permute-start(bf16[192,3072]{1,0:T(8,128)(2,1)} %slice_bitcast_fusion), channel_id=1, source_target_pairs={{0,4},{4,0},{1,5},{5,1},{2,6},{6,2},{3,7},{7,3},{8,12},{12,8},{9,1... | collective-permute-start | bytes 3538952 | tf_op jit(solution)/shard_map/ppermute | solution.py:38
  41.2 35.8 %collective-permute-start.3 = (bf16[64,3072]{1,0:T(8,128)(2,1)}, bf16[64,3072]{1,0:T(8,128)(2,1)}, u32[]{:S(2)}, u32[]{:S(2)}) collective-permute-start(bf16[64,3072]{1,0:T(8,128)(2,1)} %slice_bitcast_fusion.1), channel_id=1, source_target_pairs={{0,4},{4,0},{1,5},{5,1},{2,6},{6,2},{3,7},{7,3},{8,12},{12,8},{9,1... | collective-permute-start | bytes 1179656 | tf_op jit(solution)/shard_map/ppermute | solution.py:38
  43.1 31.4 %collective-permute-start.5 = (bf16[48,512]{1,0:T(8,128)(2,1)}, bf16[48,512]{1,0:T(8,128)(2,1)}, u32[]{:S(2)}, u32[]{:S(2)}) collective-permute-start(bf16[48,512]{1,0:T(8,128)(2,1)} %pad_maximum_fusion.5), channel_id=1, source_target_pairs={{0,4},{4,0},{1,5},{5,1},{2,6},{6,2},{3,7},{7,3},{8,12},{12,8},{9,1... | collective-permute-start | bytes 147464 | tf_op jit(solution)/shard_map/ppermute | solution.py:38
  45.1 2.9 %copy-start.32 = (bf16[3072,512]{1,0:T(8,128)(2,1)S(1)}, bf16[3072,512]{1,0:T(8,128)(2,1)}, u32[]{:S(2)}) copy-start(bf16[3072,512]{1,0:T(8,128)(2,1)} %param.25) | copy-start | bytes 9437188
  49.1 29.6 %copy-start.14 = (bf16[3072,128]{1,0:T(8,128)(2,1)S(1)}, bf16[3072,128]{1,0:T(8,128)(2,1)}, u32[]{:S(2)}) copy-start(bf16[3072,128]{1,0:T(8,128)(2,1)} %copy-done.13) | copy-start | bytes 2359300
  49.1 29.6 %copy-start.16 = (bf16[3072,128]{1,0:T(8,128)(2,1)S(1)}, bf16[3072,128]{1,0:T(8,128)(2,1)}, u32[]{:S(2)}) copy-start(bf16[3072,128]{1,0:T(8,128)(2,1)} %copy-done.15) | copy-start | bytes 2359300
  67.5 33.9 %collective-permute-start.2 = (bf16[256,256]{1,0:T(8,128)(2,1)S(1)}, bf16[256,256]{1,0:T(8,128)(2,1)S(1)}, u32[]{:S(2)}, u32[]{:S(2)}) collective-permute-start(bf16[256,256]{1,0:T(8,128)(2,1)S(1)} %convolution_convert_fusion.5.refs_0_.refs_8_), channel_id=1, source_target_pairs={{0,24},{8,0},{16,8},{24,16},{1,25},{9,1},{17,9},{25,17},{2,26},{10... | collective-permute-start | bytes 393224 | tf_op jit(solution)/shard_map/ppermute | solution.py:38
  74.5 17.0 %collective-permute-start.10 = (bf16[256,1536]{1,0:T(8,128)(2,1)S(1)}, bf16[256,1536]{1,0:T(8,128)(2,1)S(1)}, u32[]{:S(2)}, u32[]{:S(2)}) collective-permute-start(bf16[256,1536]{1,0:T(8,128)(2,1)S(1)} %constant_dynamic-slice_fusion.2), channel_id=1, source_target_pairs={{0,4},{4,0},{1,5},{5,1},{2,6},{6,2},{3,7},{7,3},{8,12},{12,8},{9,1... | collective-permute-start | bytes 2359304 | tf_op jit(solution)/shard_map/ppermute | solution.py:38
  80.9 26.7 %collective-permute-start.6 = (bf16[352,256]{1,0:T(8,128)(2,1)S(1)}, bf16[352,256]{1,0:T(8,128)(2,1)S(1)}, u32[]{:S(2)}, u32[]{:S(2)}) collective-permute-start(bf16[352,256]{1,0:T(8,128)(2,1)S(1)} %maximum_maximum_fusion.refs_4_.refs_12_), channel_id=1, source_target_pairs={{0,8},{8,16},{16,24},{24,0},{1,9},{9,17},{17,25},{25,1},{2,10},{10... | collective-permute-start | bytes 540680 | tf_op jit(solution)/shard_map/ppermute | solution.py:38
  91.5 16.1 %collective-permute-start.12 = (bf16[256,1536]{1,0:T(8,128)(2,1)S(1)}, bf16[256,1536]{1,0:T(8,128)(2,1)S(1)}, u32[]{:S(2)}, u32[]{:S(2)}) collective-permute-start(bf16[256,1536]{1,0:T(8,128)(2,1)S(1)} %collective-permute-done.10.refs_3_), channel_id=1, source_target_pairs={{0,2},{1,3},{2,0},{3,1},{4,6},{5,7},{6,4},{7,5},{8,10},{9,11},{10,... | collective-permute-start | bytes 2359304 | tf_op jit(solution)/shard_map/ppermute | solution.py:289
  95.3 12.3 %copy-start.2 = (f32[4]{0:T(128)S(1)}, f32[4]{0:T(128)}, u32[]{:S(2)}) copy-start(f32[4]{0:T(128)} %lambda_ref.3) | copy-start | bytes 52
  95.3 12.3 %copy-start.3 = (f32[128]{0:T(128)S(1)}, f32[128]{0:T(128)}, u32[]{:S(2)}) copy-start(f32[128]{0:T(128)} %param.30) | copy-start | bytes 1540
  95.4 12.2 %collective-permute-start.7 = (bf16[352,256]{1,0:T(8,128)(2,1)S(1)}, bf16[352,256]{1,0:T(8,128)(2,1)S(1)}, u32[]{:S(2)}, u32[]{:S(2)}) collective-permute-start(bf16[352,256]{1,0:T(8,128)(2,1)S(1)} %maximum_maximum_fusion.refs_4_.refs_12_), channel_id=1, source_target_pairs={{0,16},{8,24},{16,0},{24,8},{1,17},{9,25},{17,1},{25,9},{2,18},{10... | collective-permute-start | bytes 540680 | tf_op jit(solution)/shard_map/ppermute | solution.py:38
  98.7 8.9 %collective-permute-start.8 = (bf16[352,256]{1,0:T(8,128)(2,1)S(1)}, bf16[352,256]{1,0:T(8,128)(2,1)S(1)}, u32[]{:S(2)}, u32[]{:S(2)}) collective-permute-start(bf16[352,256]{1,0:T(8,128)(2,1)S(1)} %maximum_maximum_fusion.refs_4_.refs_12_), channel_id=1, source_target_pairs={{0,24},{8,0},{16,8},{24,16},{1,25},{9,1},{17,9},{25,17},{2,26},{10... | collective-permute-start | bytes 540680 | tf_op jit(solution)/shard_map/ppermute | solution.py:38
  101.4 31.8 %collective-permute-start.11 = (bf16[256,1536]{1,0:T(8,128)(2,1)S(1)}, bf16[256,1536]{1,0:T(8,128)(2,1)S(1)}, u32[]{:S(2)}, u32[]{:S(2)}) collective-permute-start(bf16[256,1536]{1,0:T(8,128)(2,1)S(1)} %collective-permute-done.10.refs_3_), channel_id=1, source_target_pairs={{0,1},{1,0},{2,3},{3,2},{4,5},{5,4},{6,7},{7,6},{8,9},{9,8},{10,11... | collective-permute-start | bytes 2359304 | tf_op jit(solution)/shard_map/ppermute | solution.py:289
  107.6 25.7 %collective-permute-start.13 = (bf16[256,1536]{1,0:T(8,128)(2,1)S(1)}, bf16[256,1536]{1,0:T(8,128)(2,1)S(1)}, u32[]{:S(2)}, u32[]{:S(2)}) collective-permute-start(bf16[256,1536]{1,0:T(8,128)(2,1)S(1)} %collective-permute-done.12.refs_5_), channel_id=1, source_target_pairs={{0,1},{1,0},{2,3},{3,2},{4,5},{5,4},{6,7},{7,6},{8,9},{9,8},{10,11... | collective-permute-start | bytes 2359304 | tf_op jit(solution)/shard_map/ppermute | solution.py:289
  119.8 13.5 %copy-start.1 = (f32[3072]{0:T(1024)S(1)}, f32[3072]{0:T(1024)}, u32[]{:S(2)}) copy-start(f32[3072]{0:T(1024)} %param.24) | copy-start | bytes 36868
  119.8 13.4 %collective-permute-start.9 = (bf16[256,512]{1,0:T(8,128)(2,1)S(1)}, bf16[256,512]{1,0:T(8,128)(2,1)S(1)}, u32[]{:S(2)}, u32[]{:S(2)}) collective-permute-start(bf16[256,512]{1,0:T(8,128)(2,1)S(1)} %shard_map.156), channel_id=1, source_target_pairs={{0,4},{4,0},{1,5},{5,1},{2,6},{6,2},{3,7},{7,3},{8,12},{12,8},{9,1... | collective-permute-start | bytes 786440 | tf_op jit(solution)/shard_map/ppermute | solution.py:38
  (15 other events, 28.8 us)
where the time goes:
time: 140 us; the launch traced here: 139 us
  Pallas kernels  50.3 us (36%)
  waiting for transfers between devices  40.2 us (29%)
  starting transfers between devices  20.4 us (15%)
  matrix products  13.4 us (10%)
  local copies, waits for them, and re-layouts  8.61 us (6%)
  other arithmetic  5.56 us (4%)
    ppermute x11, waiting for transfers between devices, shifted(): lax.ppermute(values, axis, [(i, (i + step) % size) for i in range(size)])  34.1 us
    pallas_call x2, Pallas kernels, attend(): pl.pallas_call(functools.partial(attend_kernel, len(parts)), grid=(heads,...  24.3 us
    pallas_call x1, Pallas kernels, sum_over_group(): pl.pallas_call(functools.partial(sum_kernel, sp, tp), out_shape=jax.Shape...  20.3 us
    ppermute x11, starting transfers between devices, shifted(): lax.ppermute(values, axis, [(i, (i + step) % size) for i in range(size)])  18.9 us
    dot_general x8, matrix products, project(): jnp.dot(tokens, weight, preferred_element_type=jnp.float32)  12.2 us
    ppermute x3, waiting for transfers between devices, local(): lax.ppermute(turns[turn], 'dp', [(i, i ^ bit) for i in range(dp)])  6.1 us
    pallas_call x1, Pallas kernels, tail(): pl.pallas_call(functools.partial(tail_kernel, tp, dp), out_shape=jax.Shap...  5.66 us
  transfers between devices with their start and end apart: 14, of which 4 were waited for; matrix products, arithmetic and copies ran while one was open for 12% of the time, Pallas kernels for 17%

commit v1 on v0

--- a/solution.py
+++ b/solution.py
@@ -280,9 +280,22 @@
     depth = out_weight.shape[0] // dp
     share = lax.dynamic_slice_in_dim(out_weight, lax.axis_index("dp") * depth, depth, 0)
     share, *rest = lax.optimization_barrier((share, *rest))
+    firsts = [shifted(share, "tp", tp, step) for step in steps]
+
+    other_in = modulate(
+        jnp.concatenate([part for pair in zip(heads_up, rest) for part in pair], axis=0),
+        pre_gain, shift, scale,
+    )
+    other_kv = jnp.concatenate([project(other_in, kv_weight), *contexts], axis=0)
+    other_kv = spread(other_kv)
+    other_queries = project(other_in, query_weight)
+    other_gate = project(other_in, head_gate_weight)
+
+    held = lax.optimization_barrier((*firsts, *other_kv))
+    firsts, other_kv = held[: tp - 1], list(held[tp - 1 :])
     pieces = []
-    for step in steps:
-        turns = {0: shifted(share, "tp", tp, step)}
+    for first in firsts:
+        turns = {0: first}
         bit = dp // 2
         while bit:
             for turn in list(turns):
@@ -291,14 +304,6 @@
                 )
             bit //= 2
         pieces.extend(turns[turn] for turn in range(dp))
-
-    other_in = modulate(
-        jnp.concatenate([part for pair in zip(heads_up, rest) for part in pair], axis=0),
-        pre_gain, shift, scale,
-    )
-    other_kv = spread(jnp.concatenate([project(other_in, kv_weight), *contexts], axis=0))
-    other_queries = project(other_in, query_weight)
-    other_gate = project(other_in, head_gate_weight)
 
     keys = own_kv + other_kv
     gain = head_gain[None, :]

time: 140 us -> 140 us (level)
  starting transfers between devices: 20.4 us -> 31.6 us
  waiting for transfers between devices: 40.2 us -> 29.4 us
  matrix products: 13.4 us -> 17 us
  Pallas kernels: 50.3 us -> 47.8 us
    ppermute x11, waiting for transfers between devices: 34.1 us -> 19.2 us  [shifted(): lax.ppermute(values, axis, [(i, (i + step) % size) for i in range(size)])]
    ppermute x11, starting transfers between devices: 18.9 us -> 30 us  [shifted(): lax.ppermute(values, axis, [(i, (i + step) % size) for i in range(size)])]
    ppermute x3, waiting for transfers between devices: 6.1 us -> 10.2 us  [local(): lax.ppermute(turns[turn], 'dp', [(i, i ^ bit) for i in range(dp)])]
    dot_general x8, matrix products: 12.2 us -> 15.8 us  [project(): jnp.dot(tokens, weight, preferred_element_type=jnp.float32)]
    pallas_call x1, Pallas kernels: 20.3 us -> 17.8 us  [sum_over_group(): pl.pallas_call(functools.partial(sum_kernel, sp, tp), out_shape=jax.Shape...]
  transfers between devices with their start and end apart: 14 -> 14, of which waited for: 4 -> 4; matrix products, arithmetic and copies ran while one was open for 12% -> 20% of each run, Pallas kernels for 17% -> 30%
where the time goes in v1:
time: 140 us
  Pallas kernels  47.8 us (34%)
  starting transfers between devices  31.6 us (23%)
  waiting for transfers between devices  29.4 us (21%)
  matrix products  17 us (12%)
  local copies, waits for them, and re-layouts  8.34 us (6%)
  other arithmetic  4.98 us (4%)
    ppermute x11, starting transfers between devices, shifted(): lax.ppermute(values, axis, [(i, (i + step) % size) for i in range(size)])  30 us
    pallas_call x2, Pallas kernels, attend(): pl.pallas_call(functools.partial(attend_kernel, len(parts)), grid=(heads,...  24.3 us
    ppermute x11, waiting for transfers between devices, shifted(): lax.ppermute(values, axis, [(i, (i + step) % size) for i in range(size)])  19.2 us
    pallas_call x1, Pallas kernels, sum_over_group(): pl.pallas_call(functools.partial(sum_kernel, sp, tp), out_shape=jax.Shape...  17.8 us
    dot_general x8, matrix products, project(): jnp.dot(tokens, weight, preferred_element_type=jnp.float32)  15.8 us
    ppermute x3, waiting for transfers between devices, local(): lax.ppermute(turns[turn], 'dp', [(i, i ^ bit) for i in range(dp)])  10.2 us
    pallas_call x1, Pallas kernels, tail(): pl.pallas_call(functools.partial(tail_kernel, tp, dp), out_shape=jax.Shap...  5.66 us
  transfers between devices with their start and end apart: 14, of which 4 were waited for; matrix products, arithmetic and copies ran while one was open for 20% of the time, Pallas kernels for 30%

profile of v1, /device:TPU:0, one launch (start us, length us, event | category | flops | bytes accessed | tf_op | source)
XLA Modules:
  0.0 139.5 jit_solution(14718696732296207400)
XLA Ops:
  0.0 1.9 %slice_bitcast_fusion.1 = bf16[64,3072]{1,0:T(8,128)(2,1)} fusion(bf16[1,256,3072]{2,1,0:T(8,128)(2,1)} %param.16), kind=kLoop, calls=%fused_computation.32 | loop fusion | bytes 786432 | tf_op jit(solution)/shard_map/slice | solution.py:232
  1.9 3.0 %collective-permute-start.5 = (bf16[64,3072]{1,0:T(8,128)(2,1)}, bf16[64,3072]{1,0:T(8,128)(2,1)}, u32[]{:S(2)}, u32[]{:S(2)}) collective-permute-start(bf16[64,3072]{1,0:T(8,128)(2,1)} %slice_bitcast_fusion.1), channel_id=1, source_target_pairs={{0,4},{4,0},{1,5},{5,1},{2,6},{6,2},{3,7},{7,3},{8,12},{12,8},{9,1... | collective-permute-start | bytes 1179656 | tf_op jit(solution)/shard_map/ppermute | solution.py:38
  4.9 2.4 %slice_bitcast_fusion = bf16[192,3072]{1,0:T(8,128)(2,1)} fusion(bf16[1,256,3072]{2,1,0:T(8,128)(2,1)} %param.16), kind=kLoop, calls=%fused_computation.20 | loop fusion | bytes 2359296 | tf_op jit(solution)/shard_map/slice | solution.py:245
  8.8 0.7 pad_maximum_fusion.4.part_ref
  9.5 17.8 %shard_map.154 = f32[5,3072]{1,0:T(8,128)} custom-call(f32[5,3072]{1,0:T(8,128)} %pad_maximum_fusion.4.part_ref), custom_call_target="tpu_custom_call" | custom-call | flops 1000000 | bytes 20000000 | tf_op jit(solution)/shard_map/pallas_call | solution.py:83
  27.3 1.3 fusion.31
  28.6 1.8 %convolution_convert_fusion.6 = bf16[48,256]{1,0:T(8,128)(2,1)S(1)} fusion(bf16[3072,256]{1,0:T(8,128)(2,1)} %param.27, bf16[1,48,3072]{2,1,0:T(8,128)(2,1)S(1)} %copy-done.7, f32[3072]{0:T(1024)S(1)} %bitcast.42, f32[3072]{0:T(1024)S(1)} %bitcast.44, f32[3072]{0:T(1024)S(1)} %copy-done.15, f32[48]{0:T(128)S(1)} %add_rsqrt_fusion.2), kind=kOutput, calls=%fused_computation.23 | convolution fusion | flops 76394496 | bytes 1929408 | tf_op jit(solution)/shard_map/dot_general | solution.py:34
  30.5 1.8 %convolution_convert_fusion.7 = bf16[48,256]{1,0:T(8,128)(2,1)S(1)} fusion(bf16[3072,256]{1,0:T(8,128)(2,1)} %param.26, bf16[1,48,3072]{2,1,0:T(8,128)(2,1)S(1)} %copy-done.7, f32[3072]{0:T(1024)S(1)} %bitcast.43, f32[3072]{0:T(1024)S(1)} %bitcast.45, f32[3072]{0:T(1024)S(1)} %copy-done.15, f32[48]{0:T(128)S(1)} %add_rsqrt_fusion.2), kind=kOutput, calls=%fused_computation.24 | convolution fusion | flops 76394496 | bytes 1929408 | tf_op jit(solution)/shard_map/dot_general | solution.py:34
  32.9 2.6 %collective-permute-start.6 = (bf16[48,512]{1,0:T(8,128)(2,1)}, bf16[48,512]{1,0:T(8,128)(2,1)}, u32[]{:S(2)}, u32[]{:S(2)}) collective-permute-start(bf16[48,512]{1,0:T(8,128)(2,1)} %pad_maximum_fusion.5), channel_id=1, source_target_pairs={{0,4},{4,0},{1,5},{5,1},{2,6},{6,2},{3,7},{7,3},{8,12},{12,8},{9,1... | collective-permute-start | bytes 147464 | tf_op jit(solution)/shard_map/ppermute | solution.py:38
  36.0 1.6 %constant_dynamic-slice_fusion.3 = (bf16[3072,128]{1,0:T(8,128)(2,1)S(1)}, bf16[3072,128]{1,0:T(8,128)(2,1)S(1)}) fusion(bf16[3072,256]{1,0:T(8,128)(2,1)} %param.27, s32[]{:T(128)S(6)} %select_n.18, bf16[3072,256]{1,0:T(8,128)(2,1)} %param.26), kind=kLoop, calls=%fused_computation.52 | loop fusion | bytes 3145732 | tf_op jit(solution)/shard_map/dynamic_slice | solution.py:252
  37.8 0.8 convolution_convert_fusion.5.refs_0_.refs_8_
  38.7 6.7 %collective-permute-start.2 = (bf16[256,256]{1,0:T(8,128)(2,1)S(1)}, bf16[256,256]{1,0:T(8,128)(2,1)S(1)}, u32[]{:S(2)}, u32[]{:S(2)}) collective-permute-start(bf16[256,256]{1,0:T(8,128)(2,1)S(1)} %convolution_convert_fusion.5.refs_0_.refs_8_), channel_id=1, source_target_pairs={{0,24},{8,0},{16,8},{24,16},{1,25},{9,1},{17,9},{25,17},{2,26},{10... | collective-permute-start | bytes 393224 | tf_op jit(solution)/shard_map/ppermute | solution.py:38
  45.4 3.4 %convolution_convert_fusion.2.gate_ref = bf16[256,512]{1,0:T(8,128)(2,1)S(1)} fusion(bf16[3072,512]{1,0:T(8,128)(2,1)} %param.28, bf16[1,256,3072]{2,1,0:T(8,128)(2,1)} %param.16, f32[3072]{0:T(1024)S(1)} %bitcast.47, f32[3072]{0:T(1024)S(1)} %bitcast.53, f32[3072]{0:T(1024)S(1)} %copy-done.15, f32[256]{0:T(256)S(1)} %add_rsqrt_fusion.1), kind=kOutput, calls=%fused_computation.18 | convolution fusion | flops 810156032 | bytes 5018624 | tf_op jit(solution)/shard_map/dot_general | solution.py:34
  48.8 1.3 constant_dynamic-slice_fusion.2
  50.2 0.7 constant_dynamic-slice_fusion.1
  50.9 12.4 %collective-permute-done.3 = bf16[192,3072]{1,0:T(8,128)(2,1)} collective-permute-done((bf16[192,3072]{1,0:T(8,128)(2,1)}, bf16[192,3072]{1,0:T(8,128)(2,1)}, u32[]{:S(2)}, u32[]{:S(2)}) %collective-permute-start.3) | collective-permute-done | bytes 1179680 | tf_op jit(solution)/shard_map/ppermute | solution.py:38
  63.4 1.7 %fusion = f32[256]{0:T(256)S(1)} fusion(bf16[192,3072]{1,0:T(8,128)(2,1)} %collective-permute-done.3, bf16[64,3072]{1,0:T(8,128)(2,1)} %collective-permute-done.5), kind=kLoop, calls=%fused_computation.4 | loop fusion | flops 4718336 | bytes 1573888 | tf_op jit(solution)/shard_map/reduce_sum | solution.py:23
  65.1 1.4 %collective-permute-start.4 = (bf16[256,1536]{1,0:T(8,128)(2,1)S(1)}, bf16[256,1536]{1,0:T(8,128)(2,1)S(1)}, u32[]{:S(2)}, u32[]{:S(2)}) collective-permute-start(bf16[256,1536]{1,0:T(8,128)(2,1)S(1)} %constant_dynamic-slice_fusion.2), channel_id=1, source_target_pairs={{0,4},{4,0},{1,5},{5,1},{2,6},{6,2},{3,7},{7,3},{8,12},{12,8},{9,1... | collective-permute-start | bytes 2359304 | tf_op jit(solution)/shard_map/ppermute | solution.py:38
  66.5 2.1 %convolution_convert_fusion.4 = bf16[256,256]{1,0:T(8,128)(2,1)S(1)} fusion(bf16[3072,128]{1,0:T(8,128)(2,1)S(1)} %copy-done.12, bf16[3072,128]{1,0:T(8,128)(2,1)S(1)} %copy-done.14, f32[256]{0:T(256)S(1)} %add_rsqrt_fusion, f32[3072]{0:T(1024)S(1)} %bitcast.48, f32[3072]{0:T(1024)S(1)} %bitcast.54, f32[3072]{0:T(1024)S(1)} %copy-done.15, ...), kind=kOutput, calls=%fused_computation.21 | convolution fusion | flops 412942336 | bytes 3314688 | tf_op jit(solution)/shard_map/dot_general | solution.py:34
  68.7 4.9 %collective-permute-start.9 = (bf16[352,256]{1,0:T(8,128)(2,1)S(1)}, bf16[352,256]{1,0:T(8,128)(2,1)S(1)}, u32[]{:S(2)}, u32[]{:S(2)}) collective-permute-start(bf16[352,256]{1,0:T(8,128)(2,1)S(1)} %maximum_maximum_fusion.refs_4_.refs_12_), channel_id=1, source_target_pairs={{0,24},{8,0},{16,8},{24,16},{1,25},{9,1},{17,9},{25,17},{2,26},{10... | collective-permute-start | bytes 540680 | tf_op jit(solution)/shard_map/ppermute | solution.py:38
  73.6 1.4 collective-permute-start.8
  75.0 1.0 convolution_convert_fusion.3.q_ref
  76.0 2.5 %collective-permute-done.9.refs_7_.refs_15_ = bf16[352,256]{1,0:T(8,128)(2,1)S(1)} collective-permute-done((bf16[352,256]{1,0:T(8,128)(2,1)S(1)}, bf16[352,256]{1,0:T(8,128)(2,1)S(1)}, u32[]{:S(2)}, u32[]{:S(2)}) %collective-permute-start.9) | collective-permute-done | bytes 180256 | tf_op jit(solution)/shard_map/ppermute | solution.py:38
  78.5 9.9 %collective-permute-start.1 = (bf16[256,256]{1,0:T(8,128)(2,1)S(1)}, bf16[256,256]{1,0:T(8,128)(2,1)S(1)}, u32[]{:S(2)}, u32[]{:S(2)}) collective-permute-start(bf16[256,256]{1,0:T(8,128)(2,1)S(1)} %convolution_convert_fusion.5.refs_0_.refs_8_), channel_id=1, source_target_pairs={{0,16},{8,24},{16,0},{24,8},{1,17},{9,25},{17,1},{25,9},{2,18},{10... | collective-permute-start | bytes 393224 | tf_op jit(solution)/shard_map/ppermute | solution.py:38
  88.5 4.2 %collective-permute-done.8.refs_6_.refs_14_ = bf16[352,256]{1,0:T(8,128)(2,1)S(1)} collective-permute-done((bf16[352,256]{1,0:T(8,128)(2,1)S(1)}, bf16[352,256]{1,0:T(8,128)(2,1)S(1)}, u32[]{:S(2)}, u32[]{:S(2)}) %collective-permute-start.8) | collective-permute-done | bytes 180256 | tf_op jit(solution)/shard_map/ppermute | solution.py:38
  92.7 1.6 %collective-permute-start.12 = (bf16[256,1536]{1,0:T(8,128)(2,1)S(1)}, bf16[256,1536]{1,0:T(8,128)(2,1)S(1)}, u32[]{:S(2)}, u32[]{:S(2)}) collective-permute-start(bf16[256,1536]{1,0:T(8,128)(2,1)S(1)} %collective-permute-done.4.refs_3_), channel_id=1, source_target_pairs={{0,2},{1,3},{2,0},{3,1},{4,6},{5,7},{6,4},{7,5},{8,10},{9,11},{10,... | collective-permute-start | bytes 2359304 | tf_op jit(solution)/shard_map/ppermute | solution.py:302
  94.2 2.4 %convolution_convert_fusion.1.q_ref = bf16[256,512]{1,0:T(8,128)(2,1)S(1)} fusion(bf16[3072,512]{1,0:T(8,128)(2,1)S(1)} %copy-done, f32[256]{0:T(256)S(1)} %add_rsqrt_fusion, f32[3072]{0:T(1024)S(1)} %bitcast.50, f32[3072]{0:T(1024)S(1)} %bitcast.56, f32[3072]{0:T(1024)S(1)} %copy-done.15, bf16[192,3072]{1,0:T(8,128)(2,1)} %collective-permute-done.3, ...), kind=kOutput, calls=%fused_computation.17 | convolution fusion | flops 812515328 | bytes 5018624 | tf_op jit(solution)/shard_map/dot_general | solution.py:34
  96.7 2.4 %convolution_convert_fusion.gate_ref = bf16[256,512]{1,0:T(8,128)(2,1)S(1)} fusion(bf16[3072,512]{1,0:T(8,128)(2,1)S(1)} %copy-done.18, f32[256]{0:T(256)S(1)} %add_rsqrt_fusion, f32[3072]{0:T(1024)S(1)} %bitcast.51, f32[3072]{0:T(1024)S(1)} %bitcast.57, f32[3072]{0:T(1024)S(1)} %copy-done.15, bf16[192,3072]{1,0:T(8,128)(2,1)} %collective-permute-done.3, ...), kind=kOutput, calls=%fused_computation.16 | convolution fusion | flops 812515328 | bytes 5018624 | tf_op jit(solution)/shard_map/dot_general | solution.py:34
  99.1 10.2 %collective-permute-done.12.refs_5_ = bf16[256,1536]{1,0:T(8,128)(2,1)S(1)} collective-permute-done((bf16[256,1536]{1,0:T(8,128)(2,1)S(1)}, bf16[256,1536]{1,0:T(8,128)(2,1)S(1)}, u32[]{:S(2)}, u32[]{:S(2)}) %collective-permute-start.12) | collective-permute-done | bytes 786464 | tf_op jit(solution)/shard_map/ppermute | solution.py:302
  109.4 12.2 %shard_map.156 = bf16[256,512]{1,0:T(8,128)(2,1)S(1)} custom-call(f32[4]{0:T(128)S(1)} %copy-done.2, bf16[256,512]{1,0:T(8,128)(2,1)S(1)} %convolution_convert_fusion.1.q_ref, bf16[256,512]{1,0:T(8,128)(2,1)S(1)} %convolution_convert_fusion.gate_ref, f32[1,128]{1,0:T(1,128)S(1)} %bitcast.40, bf16[256,256]{1,0:T(8,128)(2,1)S(1)} %convolution_convert_fusion.5.refs_0_.refs_8_, ...), custom_call_target="tpu_custom_call" | custom-call | flops 5100273664 | bytes 4000000 | tf_op jit(solution)/shard_map/pallas_call | solution.py:131
  121.7 12.2 %shard_map.155.refs_0_ = bf16[256,512]{1,0:T(8,128)(2,1)S(1)} custom-call(f32[4]{0:T(128)S(1)} %copy-done.2, bf16[256,512]{1,0:T(8,128)(2,1)S(1)} %convolution_convert_fusion.3.q_ref, bf16[256,512]{1,0:T(8,128)(2,1)S(1)} %convolution_convert_fusion.2.gate_ref, f32[1,128]{1,0:T(1,128)S(1)} %bitcast.41, ...), custom_call_target="tpu_custom_call" | custom-call | flops 5100273664 | bytes 4000000 | tf_op jit(solution)/shard_map/pallas_call | solution.py:131
  133.9 5.7 %shard_map.157 = bf16[256,3072]{1,0:T(8,128)(2,1)} custom-call(bf16[256,512]{1,0:T(8,128)(2,1)S(1)} %shard_map.155.refs_0_, bf16[256,512]{1,0:T(8,128)(2,1)S(1)} %collective-permute-done.10.refs_1_, bf16[1024,1536]{1,0:T(8,128)(2,1)} %refs_2_.1, bf16[256,1536]{1,0:T(8,128)(2,1)S(1)} %collective-permute-done.4.refs_3_, ...), custom_call_target="tpu_custom_call" | custom-call | flops 1610612736 | bytes 10000000 | tf_op jit(solution)/shard_map/pallas_call | solution.py:187
  (67 shorter events, 3.2 us)
Async XLA Ops:
  0.0 75.0 %copy-start = (bf16[3072,512]{1,0:T(8,128)(2,1)S(1)}, bf16[3072,512]{1,0:T(8,128)(2,1)}, u32[]{:S(2)}) copy-start(bf16[3072,512]{1,0:T(8,128)(2,1)} %param.25) | copy-start | bytes 9437188
  0.0 7.3 %copy-start.7 = (bf16[1,48,3072]{2,1,0:T(8,128)(2,1)S(1)}, bf16[1,48,3072]{2,1,0:T(8,128)(2,1)}, u32[]{:S(2)}) copy-start(bf16[1,48,3072]{2,1,0:T(8,128)(2,1)} %param.18) | copy-start | bytes 884740
  0.0 7.5 %copy-start.17 = (bf16[384]{0:T(512)(128)(2,1)S(1)}, bf16[384]{0:T(512)(128)(2,1)}, u32[]{:S(2)}) copy-start(bf16[384]{0:T(512)(128)(2,1)} %param.19) | copy-start | bytes 2308
  0.0 7.5 %copy-start.16 = (bf16[1,384]{1,0:T(2,128)(2,1)S(1)}, bf16[1,384]{1,0:T(2,128)(2,1)}, u32[]{:S(2)}) copy-start(bf16[1,384]{1,0:T(2,128)(2,1)} %param.17) | copy-start | bytes 2308
  0.0 7.5 %copy-start.8 = (bf16[384,3072]{1,0:T(8,128)(2,1)S(1)}, bf16[384,3072]{1,0:T(8,128)(2,1)}, u32[]{:S(2)}) copy-start(bf16[384,3072]{1,0:T(8,128)(2,1)} %param.22) | copy-start | bytes 7077892
  0.0 7.9 %copy-start.9 = (bf16[384,3072]{1,0:T(8,128)(2,1)S(1)}, bf16[384,3072]{1,0:T(8,128)(2,1)}, u32[]{:S(2)}) copy-start(bf16[384,3072]{1,0:T(8,128)(2,1)} %param.21) | copy-start | bytes 7077892
  1.9 6.5 %copy-start.10 = (bf16[384,3072]{1,0:T(8,128)(2,1)S(1)}, bf16[384,3072]{1,0:T(8,128)(2,1)}, u32[]{:S(2)}) copy-start(bf16[384,3072]{1,0:T(8,128)(2,1)} %param.20) | copy-start | bytes 7077892
  1.9 61.4 %collective-permute-start.5 = (bf16[64,3072]{1,0:T(8,128)(2,1)}, bf16[64,3072]{1,0:T(8,128)(2,1)}, u32[]{:S(2)}, u32[]{:S(2)}) collective-permute-start(bf16[64,3072]{1,0:T(8,128)(2,1)} %slice_bitcast_fusion.1), channel_id=1, source_target_pairs={{0,4},{4,0},{1,5},{5,1},{2,6},{6,2},{3,7},{7,3},{8,12},{12,8},{9,1... | collective-permute-start | bytes 1179656 | tf_op jit(solution)/shard_map/ppermute | solution.py:38
  8.0 20.6 %copy-start.15 = (f32[3072]{0:T(1024)S(1)}, f32[3072]{0:T(1024)}, u32[]{:S(2)}) copy-start(f32[3072]{0:T(1024)} %param.23) | copy-start | bytes 36868
  27.3 8.2 %copy-start.4 = (bf16[1,256,3072]{2,1,0:T(8,128)(2,1)S(1)}, bf16[1,256,3072]{2,1,0:T(8,128)(2,1)}, u32[]{:S(2)}) copy-start(bf16[1,256,3072]{2,1,0:T(8,128)(2,1)} %param.16) | copy-start | bytes 4718596
  32.9 17.3 %collective-permute-start.6 = (bf16[48,512]{1,0:T(8,128)(2,1)}, bf16[48,512]{1,0:T(8,128)(2,1)}, u32[]{:S(2)}, u32[]{:S(2)}) collective-permute-start(bf16[48,512]{1,0:T(8,128)(2,1)} %pad_maximum_fusion.5), channel_id=1, source_target_pairs={{0,4},{4,0},{1,5},{5,1},{2,6},{6,2},{3,7},{7,3},{8,12},{12,8},{9,1... | collective-permute-start | bytes 147464 | tf_op jit(solution)/shard_map/ppermute | solution.py:38
  35.5 27.8 %collective-permute-start.3 = (bf16[192,3072]{1,0:T(8,128)(2,1)}, bf16[192,3072]{1,0:T(8,128)(2,1)}, u32[]{:S(2)}, u32[]{:S(2)}) collective-permute-start(bf16[192,3072]{1,0:T(8,128)(2,1)} %slice_bitcast_fusion), channel_id=1, source_target_pairs={{0,4},{4,0},{1,5},{5,1},{2,6},{6,2},{3,7},{7,3},{8,12},{12,8},{9,1... | collective-permute-start | bytes 3538952 | tf_op jit(solution)/shard_map/ppermute | solution.py:38
  36.0 1.9 %copy-start.5 = (bf16[1,256,3072]{2,1,0:T(8,128)(2,1)S(1)}, bf16[1,256,3072]{2,1,0:T(8,128)(2,1)}, u32[]{:S(2)}) copy-start(bf16[1,256,3072]{2,1,0:T(8,128)(2,1)} %param.16) | copy-start | bytes 4718596
  37.6 1.1 copy-start.13
  38.7 70.6 %collective-permute-start.2 = (bf16[256,256]{1,0:T(8,128)(2,1)S(1)}, bf16[256,256]{1,0:T(8,128)(2,1)S(1)}, u32[]{:S(2)}, u32[]{:S(2)}) collective-permute-start(bf16[256,256]{1,0:T(8,128)(2,1)S(1)} %convolution_convert_fusion.5.refs_0_.refs_8_), channel_id=1, source_target_pairs={{0,24},{8,0},{16,8},{24,16},{1,25},{9,1},{17,9},{25,17},{2,26},{10... | collective-permute-start | bytes 393224 | tf_op jit(solution)/shard_map/ppermute | solution.py:38
  48.8 17.7 %copy-start.12 = (bf16[3072,128]{1,0:T(8,128)(2,1)S(1)}, bf16[3072,128]{1,0:T(8,128)(2,1)}, u32[]{:S(2)}) copy-start(bf16[3072,128]{1,0:T(8,128)(2,1)} %copy-done.11) | copy-start | bytes 2359300
  48.8 17.7 %copy-start.14 = (bf16[3072,128]{1,0:T(8,128)(2,1)S(1)}, bf16[3072,128]{1,0:T(8,128)(2,1)}, u32[]{:S(2)}) copy-start(bf16[3072,128]{1,0:T(8,128)(2,1)} %copy-done.13) | copy-start | bytes 2359300
  65.1 9.9 %copy-start.6 = (bf16[1,256,3072]{2,1,0:T(8,128)(2,1)S(1)}, bf16[1,256,3072]{2,1,0:T(8,128)(2,1)}, u32[]{:S(2)}) copy-start(bf16[1,256,3072]{2,1,0:T(8,128)(2,1)} %param.16) | copy-start | bytes 4718596
  65.1 27.5 %collective-permute-start.4 = (bf16[256,1536]{1,0:T(8,128)(2,1)S(1)}, bf16[256,1536]{1,0:T(8,128)(2,1)S(1)}, u32[]{:S(2)}, u32[]{:S(2)}) collective-permute-start(bf16[256,1536]{1,0:T(8,128)(2,1)S(1)} %constant_dynamic-slice_fusion.2), channel_id=1, source_target_pairs={{0,4},{4,0},{1,5},{5,1},{2,6},{6,2},{3,7},{7,3},{8,12},{12,8},{9,1... | collective-permute-start | bytes 2359304 | tf_op jit(solution)/shard_map/ppermute | solution.py:38
  68.7 9.9 %collective-permute-start.9 = (bf16[352,256]{1,0:T(8,128)(2,1)S(1)}, bf16[352,256]{1,0:T(8,128)(2,1)S(1)}, u32[]{:S(2)}, u32[]{:S(2)}) collective-permute-start(bf16[352,256]{1,0:T(8,128)(2,1)S(1)} %maximum_maximum_fusion.refs_4_.refs_12_), channel_id=1, source_target_pairs={{0,24},{8,0},{16,8},{24,16},{1,25},{9,1},{17,9},{25,17},{2,26},{10... | collective-permute-start | bytes 540680 | tf_op jit(solution)/shard_map/ppermute | solution.py:38
  73.6 19.1 %collective-permute-start.8 = (bf16[352,256]{1,0:T(8,128)(2,1)S(1)}, bf16[352,256]{1,0:T(8,128)(2,1)S(1)}, u32[]{:S(2)}, u32[]{:S(2)}) collective-permute-start(bf16[352,256]{1,0:T(8,128)(2,1)S(1)} %maximum_maximum_fusion.refs_4_.refs_12_), channel_id=1, source_target_pairs={{0,16},{8,24},{16,0},{24,8},{1,17},{9,25},{17,1},{25,9},{2,18},{10... | collective-permute-start | bytes 540680 | tf_op jit(solution)/shard_map/ppermute | solution.py:38
  75.0 17.7 %collective-permute-start.7 = (bf16[352,256]{1,0:T(8,128)(2,1)S(1)}, bf16[352,256]{1,0:T(8,128)(2,1)S(1)}, u32[]{:S(2)}, u32[]{:S(2)}) collective-permute-start(bf16[352,256]{1,0:T(8,128)(2,1)S(1)} %maximum_maximum_fusion.refs_4_.refs_12_), channel_id=1, source_target_pairs={{0,8},{8,16},{16,24},{24,0},{1,9},{9,17},{17,25},{25,1},{2,10},{10... | collective-permute-start | bytes 540680 | tf_op jit(solution)/shard_map/ppermute | solution.py:38
  76.0 20.6 %copy-start.18 = (bf16[3072,512]{1,0:T(8,128)(2,1)S(1)}, bf16[3072,512]{1,0:T(8,128)(2,1)}, u32[]{:S(2)}) copy-start(bf16[3072,512]{1,0:T(8,128)(2,1)} %param.28) | copy-start | bytes 9437188
  78.5 30.8 %collective-permute-start.1 = (bf16[256,256]{1,0:T(8,128)(2,1)S(1)}, bf16[256,256]{1,0:T(8,128)(2,1)S(1)}, u32[]{:S(2)}, u32[]{:S(2)}) collective-permute-start(bf16[256,256]{1,0:T(8,128)(2,1)S(1)} %convolution_convert_fusion.5.refs_0_.refs_8_), channel_id=1, source_target_pairs={{0,16},{8,24},{16,0},{24,8},{1,17},{9,25},{17,1},{25,9},{2,18},{10... | collective-permute-start | bytes 393224 | tf_op jit(solution)/shard_map/ppermute | solution.py:38
  92.7 16.7 %collective-permute-start = (bf16[256,256]{1,0:T(8,128)(2,1)S(1)}, bf16[256,256]{1,0:T(8,128)(2,1)S(1)}, u32[]{:S(2)}, u32[]{:S(2)}) collective-permute-start(bf16[256,256]{1,0:T(8,128)(2,1)S(1)} %convolution_convert_fusion.5.refs_0_.refs_8_), channel_id=1, source_target_pairs={{0,8},{8,16},{16,24},{24,0},{1,9},{9,17},{17,25},{25,1},{2,10},{10... | collective-permute-start | bytes 393224 | tf_op jit(solution)/shard_map/ppermute | solution.py:38
  92.7 16.7 %collective-permute-start.12 = (bf16[256,1536]{1,0:T(8,128)(2,1)S(1)}, bf16[256,1536]{1,0:T(8,128)(2,1)S(1)}, u32[]{:S(2)}, u32[]{:S(2)}) collective-permute-start(bf16[256,1536]{1,0:T(8,128)(2,1)S(1)} %collective-permute-done.4.refs_3_), channel_id=1, source_target_pairs={{0,2},{1,3},{2,0},{3,1},{4,6},{5,7},{6,4},{7,5},{8,10},{9,11},{10,... | collective-permute-start | bytes 2359304 | tf_op jit(solution)/shard_map/ppermute | solution.py:302
  96.6 12.8 %copy-start.2 = (f32[4]{0:T(128)S(1)}, f32[4]{0:T(128)}, u32[]{:S(2)}) copy-start(f32[4]{0:T(128)} %lambda_ref.3) | copy-start | bytes 52
  96.6 12.8 %copy-start.3 = (f32[128]{0:T(128)S(1)}, f32[128]{0:T(128)}, u32[]{:S(2)}) copy-start(f32[128]{0:T(128)} %param.30) | copy-start | bytes 1540
  99.1 34.8 %collective-permute-start.11 = (bf16[256,1536]{1,0:T(8,128)(2,1)S(1)}, bf16[256,1536]{1,0:T(8,128)(2,1)S(1)}, u32[]{:S(2)}, u32[]{:S(2)}) collective-permute-start(bf16[256,1536]{1,0:T(8,128)(2,1)S(1)} %collective-permute-done.4.refs_3_), channel_id=1, source_target_pairs={{0,1},{1,0},{2,3},{3,2},{4,5},{5,4},{6,7},{7,6},{8,9},{9,8},{10,11... | collective-permute-start | bytes 2359304 | tf_op jit(solution)/shard_map/ppermute | solution.py:302
  109.4 24.5 %collective-permute-start.13 = (bf16[256,1536]{1,0:T(8,128)(2,1)S(1)}, bf16[256,1536]{1,0:T(8,128)(2,1)S(1)}, u32[]{:S(2)}, u32[]{:S(2)}) collective-permute-start(bf16[256,1536]{1,0:T(8,128)(2,1)S(1)} %collective-permute-done.12.refs_5_), channel_id=1, source_target_pairs={{0,1},{1,0},{2,3},{3,2},{4,5},{5,4},{6,7},{7,6},{8,9},{9,8},{10,11... | collective-permute-start | bytes 2359304 | tf_op jit(solution)/shard_map/ppermute | solution.py:302
  121.6 12.3 %copy-start.1 = (f32[3072]{0:T(1024)S(1)}, f32[3072]{0:T(1024)}, u32[]{:S(2)}) copy-start(f32[3072]{0:T(1024)} %param.24) | copy-start | bytes 36868
  121.6 12.3 %collective-permute-start.10 = (bf16[256,512]{1,0:T(8,128)(2,1)S(1)}, bf16[256,512]{1,0:T(8,128)(2,1)S(1)}, u32[]{:S(2)}, u32[]{:S(2)}) collective-permute-start(bf16[256,512]{1,0:T(8,128)(2,1)S(1)} %shard_map.156), channel_id=1, source_target_pairs={{0,4},{4,0},{1,5},{5,1},{2,6},{6,2},{3,7},{7,3},{8,12},{12,8},{9,1... | collective-permute-start | bytes 786440 | tf_op jit(solution)/shard_map/ppermute | solution.py:38
  (1 other events, 1.1 us)
